TPU v7x, 32 devices: a whole 2x2x4 slice. The times are simulated.
32 devices in a mesh: grp: 2 (over y), fs: 4 (over z), tp: 4 (over x, core).
Axes of the slice: x: 2, y: 2, z: 4, core: 2. Of those that a mesh axis runs over, the one named last changes fastest.
Arguments:
- residual_in: bfloat16 [4096, 2048], P(('grp', 'fs', 'tp')), parts along dimension 0, may hold values from -6 to 6
- hidden_first: bfloat16 [4096, 5632], P(('grp', 'fs', 'tp')), parts along dimension 0, may hold values from -6 to 6
- down_weight: bfloat16 [5632, 2048], P('tp', 'fs'), may hold values from -0.078125 to 0.078125
- mixer_out: bfloat16 [4096, 2048], P(('grp', 'fs', 'tp')), parts along dimension 0, may hold values from -6 to 6
- norm_gain: float32 [2, 2048], replicated, may hold values from 0.1 to 1.9
- norm_shift: float32 [2, 2048], replicated, may hold values from -1.5 to 1.5
- gate_weight: bfloat16 [2048, 5632], P('fs', 'tp'), may hold values from -0.125 to 0.125
- up_weight: bfloat16 [2048, 5632], P('fs', 'tp'), may hold values from -0.125 to 0.125
Outputs:
- mixed_state: bfloat16 [4096, 2048], P(('grp', 'fs', 'tp')), parts along dimension 0
- hidden_second: bfloat16 [4096, 5632], P(('grp', 'fs'), 'tp'), parts along dimension 0
There are 2 independent parts, one for each index of `grp`. A program takes and returns all parts, laid end to end along the dimension named above; an argument that names none is the same for every part. Nothing has to cross between parts.
All inputs are finite; a program needn't handle non-finite values.
Results may differ from a plain program's by a relative error of at most 0.012.
Values may be sent and summed in bfloat16 or wider, within the bound.
A program may use at most 64 MiB of HBM per device.

v0:
```python
import jax
import jax.numpy as jnp
from jax import lax
from jax.sharding import PartitionSpec as P


def layer_norm(values, gain, shift):
    center = values - jnp.mean(values, axis=-1, keepdims=True)
    variance = jnp.mean(center * center, axis=-1, keepdims=True)
    return center * lax.rsqrt(variance + 1e-05) * gain + shift


def on_device(
    residual_in, hidden_first, down_weight, mixer_out, norm_gain, norm_shift, gate_weight, up_weight
):
    spread = lax.all_to_all(hidden_first, "tp", split_axis=1, concat_axis=0, tiled=True)
    down_full = lax.all_gather(down_weight, "fs", axis=1, tiled=True)
    branch = lax.psum_scatter(
        jnp.dot(spread, down_full, preferred_element_type=jnp.float32).astype(jnp.bfloat16),
        "tp",
        scatter_dimension=0,
        tiled=True,
    ).astype(jnp.float32)
    first = layer_norm(
        jnp.sqrt(2.0) * residual_in.astype(jnp.float32) + 0.5 * branch, norm_gain[0], norm_shift[0]
    )
    mixed_state = layer_norm(
        jnp.sqrt(2.0) * first + mixer_out.astype(jnp.float32), norm_gain[1], norm_shift[1]
    ).astype(jnp.bfloat16)
    gathered = lax.all_gather(mixed_state, "tp", axis=0, tiled=True)
    width = gate_weight.shape[1]
    joined = jnp.concatenate([gate_weight, up_weight], axis=1)
    both = jnp.dot(
        gathered,
        lax.all_gather(joined, "fs", axis=0, tiled=True),
        preferred_element_type=jnp.float32,
    )
    gate = both[:, :width]
    up = both[:, width:]
    hidden_second = (jax.nn.silu(gate) * up).astype(jnp.bfloat16)
    return (mixed_state, hidden_second)


def solution(mesh):
    in_specs = (
        P(("grp", "fs", "tp"), None),
        P(("grp", "fs", "tp"), None),
        P("tp", "fs"),
        P(("grp", "fs", "tp"), None),
        P(),
        P(),
        P("fs", "tp"),
        P("fs", "tp"),
    )
    out_specs = (P(("grp", "fs", "tp"), None), P(("grp", "fs"), "tp"))
    return jax.shard_map(
        on_device, mesh=mesh, in_specs=in_specs, out_specs=out_specs, check_vma=False
    )
```

profile of v0, /device:TPU:0, one launch (start us, length us, event | category | flops | bytes accessed | tf_op | source)
XLA Modules:
  0.0 405.8 jit_solution(10597806756419352990)
XLA Ops:
  7.2 0.0 all-gather.4.cloned.1.call-start
  7.2 0.7 all-gather.4.cloned.1.call-update
  7.9 0.0 reduce-scatter.2.cloned.1.call-start
  7.9 1.8 copy.10
  9.8 22.7 %all_to_all.19 = bf16[128,4,1408]{0,2,1:T(8,128)(2,1)S(1)} all-to-all(bf16[128,4,1408]{0,2,1:T(8,128)(2,1)S(1)} %bitcast.12), channel_id=1, replica_groups=mesh['grp'=2,'fs'=4,'tp'=4] {'tp'}, dimensions={1} | all-to-all | bytes 2883584 | tf_op jit(solution)/shard_map/all_to_all | solution.py:16
  32.5 0.8 copy.11
  33.3 85.7 %all-gather.4.cloned.1.call-done = bf16[1408,2048]{1,0:T(8,128)(2,1)} async-done(((bf16[1408,512]{1,0:T(8,128)(2,1)}), bf16[1408,2048]{1,0:T(8,128)(2,1)}) %all-gather.4.cloned.1.call-update) | async-done | bytes 5767184 | tf_op jit(solution)/shard_map/all_gather | solution.py:17
  119.0 0.0 copy-start.3
  119.0 0.0 copy-start.4
  119.0 7.2 %convolution_convert_fusion = bf16[512,2048]{1,0:T(8,128)(2,1)} fusion(bf16[512,1408]{1,0:T(8,128)(2,1)S(1)} %bitcast.13, bf16[1408,2048]{1,0:T(8,128)(2,1)} %all-gather.4.cloned.1.call-done), kind=kOutput, calls=%fused_computation | convolution fusion | flops 2953838592 | bytes 9306112 | tf_op jit(solution)/shard_map/dot_general | solution.py:19
  126.2 0.0 reduce-scatter.2.cloned.1.call-update
  126.3 0.0 all-gather.6.cloned.1.call-start
  126.3 0.0 copy-done.3
  126.3 0.0 copy-done.4
  126.4 29.5 %reduce-scatter.2.cloned.1.call-done = bf16[128,2048]{1,0:T(8,128)(2,1)} async-done(((bf16[512,2048]{1,0:T(8,128)(2,1)}), bf16[128,2048]{1,0:T(8,128)(2,1)}) %reduce-scatter.2.cloned.1.call-update) | async-done | bytes 524304 | tf_op jit(solution)/shard_map/reduce_scatter | solution.py:18
  155.9 0.0 copy-done
  155.9 1.3 fusion.1
  157.2 1.4 multiply_reduce_fusion.1
  158.6 0.0 copy-start.2
  158.6 1.9 fusion.2
  160.5 0.3 multiply_reduce_fusion
  160.8 1.1 add_convert_fusion
  161.8 0.0 all-gather.6.cloned.1.call-update
  161.9 0.0 all-gather.8.cloned.1.call-start
  161.9 0.0 copy-done.1
  161.9 0.0 copy-done.2
  161.9 1.9 pad_maximum_fusion
  163.8 0.0 all-gather.8.cloned.1.call-update
  163.8 20.8 %all-gather.6.cloned.1.call-done = bf16[512,2048]{1,0:T(8,128)(2,1)} async-done(((bf16[128,2048]{1,0:T(8,128)(2,1)}), bf16[512,2048]{1,0:T(8,128)(2,1)}) %all-gather.6.cloned.1.call-update) | async-done | bytes 2097168 | tf_op jit(solution)/shard_map/all_gather | solution.py:30
  184.6 202.5 %all-gather.8.cloned.1.call-done = bf16[2048,2816]{1,0:T(8,128)(2,1)} async-done(((bf16[512,2816]{1,0:T(8,128)(2,1)}), bf16[2048,2816]{1,0:T(8,128)(2,1)}) %all-gather.8.cloned.1.call-update) | async-done | bytes 11534352 | tf_op jit(solution)/shard_map/all_gather | solution.py:35
  387.1 10.2 %fusion.5 = f32[512,2816]{1,0:T(8,128)S(1)} fusion(bf16[512,2048]{1,0:T(8,128)(2,1)} %all-gather.6.cloned.1.call-done, bf16[2048,2816]{1,0:T(8,128)(2,1)} %all-gather.8.cloned.1.call-done), kind=kOutput, calls=%fused_computation.17 | convolution fusion | flops 5905580032 | bytes 19398656 | tf_op jit(solution)/shard_map/dot_general | solution.py:33
  397.3 2.0 fusion
  (8 shorter events, 0.1 us)
Async XLA Ops:
  7.2 111.8 %all-gather.4.cloned.1.call-start = ((), (), s32[]{:S(2)}) async-start(), calls=%async_computation.2 | async-start | bytes 7208960 | tf_op jit(solution)/shard_map/all_gather | solution.py:17
  7.9 148.0 %reduce-scatter.2.cloned.1.call-start = ((), (), s32[]{:S(2)}) async-start(), calls=%async_computation.3 | async-start | bytes 2621440 | tf_op jit(solution)/shard_map/reduce_scatter | solution.py:18
  119.0 7.3 %copy-start.3 = (f32[2,2048]{1,0:T(2,128)S(1)}, f32[2,2048]{1,0:T(2,128)}, u32[]{:S(2)}) copy-start(f32[2,2048]{1,0:T(2,128)} %param.12) | copy-start | bytes 49156
  119.0 7.4 %copy-start.4 = (f32[2,2048]{1,0:T(2,128)S(1)}, f32[2,2048]{1,0:T(2,128)}, u32[]{:S(2)}) copy-start(f32[2,2048]{1,0:T(2,128)} %param.13) | copy-start | bytes 49156
  119.0 36.9 %copy-start = (bf16[128,2048]{1,0:T(8,128)(2,1)S(1)}, bf16[128,2048]{1,0:T(8,128)(2,1)}, u32[]{:S(2)}) copy-start(bf16[128,2048]{1,0:T(8,128)(2,1)} %param.8) | copy-start | bytes 1572868
  126.3 58.3 %all-gather.6.cloned.1.call-start = ((), (), s32[]{:S(2)}) async-start(), calls=%async_computation.4 | async-start | bytes 2621440 | tf_op jit(solution)/shard_map/all_gather | solution.py:30
  158.6 3.3 copy-start.1
  158.6 3.3 copy-start.2
  161.9 225.2 %all-gather.8.cloned.1.call-start = ((), (), s32[]{:S(2)}) async-start(), calls=%async_computation.5 | async-start | bytes 14417920 | tf_op jit(solution)/shard_map/all_gather | solution.py:35
Sparse Core Ops, SparseCore 0:
  9.5 109.3 all-gather.3
  126.4 29.4 reduce-scatter.1
  162.0 22.5 all-gather.5
  186.0 201.0 all-gather.7
where the time goes:
time: 406 us
  waiting for transfers between devices  339 us (83%)
  blocking collectives  22.7 us (6%)
  matrix products  17.4 us (4%)
  between operations  13.9 us (3%)
  other arithmetic  9.78 us (2%)
    all_gather x1, waiting for transfers between devices, on_device(): lax.all_gather(joined, 'fs', axis=0, tiled=True)  202 us
    all_gather x1, waiting for transfers between devices, on_device(): down_full = lax.all_gather(down_weight, 'fs', axis=1, tiled=True)  85.7 us
    reduce_scatter x1, waiting for transfers between devices, on_device(): lax.psum_scatter(jnp.dot(spread, down_full, preferred_element_type=jnp.fl...  29.5 us
    all_to_all x1, blocking collectives, on_device(): lax.all_to_all(hidden_first, 'tp', split_axis=1, concat_axis=0, tiled=True)  22.7 us
    all_gather x1, waiting for transfers between devices, on_device(): gathered = lax.all_gather(mixed_state, 'tp', axis=0, tiled=True)  20.8 us
    dot_general x1, matrix products, on_device(): jnp.dot(gathered, lax.all_gather(joined, 'fs', axis=0, tiled=True), prefe...  10.2 us
  transfers between devices with their start and end apart: 4, of which 4 were waited for; matrix products, arithmetic and copies ran while one was open for 1% of the time, Pallas kernels for 0%

commit v1 on v0

--- a/solution.py
+++ b/solution.py
@@ -2,6 +2,13 @@
 import jax.numpy as jnp
 from jax import lax
 from jax.sharding import PartitionSpec as P
+
+
+def patch_trace(axis_id, payload):
+    current_arr = jnp.concatenate(
+        lax.all_to_all(jnp.stack(lax.axis_size(axis_id) * [payload]), axis_id, 0, 0), 0
+    )
+    return current_arr
 
 
 def layer_norm(values, gain, shift):
@@ -30,11 +37,7 @@
     gathered = lax.all_gather(mixed_state, "tp", axis=0, tiled=True)
     width = gate_weight.shape[1]
     joined = jnp.concatenate([gate_weight, up_weight], axis=1)
-    both = jnp.dot(
-        gathered,
-        lax.all_gather(joined, "fs", axis=0, tiled=True),
-        preferred_element_type=jnp.float32,
-    )
+    both = jnp.dot(gathered, patch_trace("fs", payload=joined), preferred_element_type=jnp.float32)
     gate = both[:, :width]
     up = both[:, width:]
     hidden_second = (jax.nn.silu(gate) * up).astype(jnp.bfloat16)

time: 406 us -> 385 us (0.948)
  blocking collectives: 22.7 us -> 0 us
  waiting for transfers between devices: 339 us -> 323 us
  starting transfers between devices: 0.16 us -> 10.6 us
  local copies, waits for them, and re-layouts: 2.69 us -> 9.34 us
    all_gather x1 -> x0, waiting for transfers between devices: 202 us -> none  [on_device(): lax.all_gather(joined, 'fs', axis=0, tiled=True)]
    all_to_all x0 -> x2, waiting for transfers between devices: none -> 103 us  [the longest x1 85.1 us: patch_trace(): lax.all_to_all(jnp.stack(lax.axis_size(axis_id) * [payload]), axis_id, 0, 0)]
    all_gather x1, waiting for transfers between devices: 85.7 us -> 168 us  [on_device(): down_full = lax.all_gather(down_weight, 'fs', axis=1, tiled=True)]
    all_to_all x1 -> x0, blocking collectives: 22.7 us -> none  [on_device(): lax.all_to_all(hidden_first, 'tp', split_axis=1, concat_axis=0, tiled=True)]
    all_to_all x0 -> x2, starting transfers between devices: none -> 10.5 us  [the longest x1 6.15 us: patch_trace(): lax.all_to_all(jnp.stack(lax.axis_size(axis_id) * [payload]), axis_id, 0, 0)]
    another operation x0 -> x1, local copies, waits for them, and re-layouts: none -> 4.95 us  [patch_trace(): jnp.stack(lax.axis_size(axis_id) * [payload])]
  transfers between devices with their start and end apart: 4 -> 5, of which waited for: 4 -> 5; matrix products, arithmetic and copies ran while one was open for 1% -> 6% of each run, Pallas kernels for 0% -> 0%
where the time goes in v1:
time: 385 us; the launch traced here: 384 us
  waiting for transfers between devices  323 us (84%)
  matrix products  17.4 us (5%)
  between operations  13.8 us (4%)
  starting transfers between devices  10.6 us (3%)
  other arithmetic  9.61 us (2%)
  local copies, waits for them, and re-layouts  9.34 us (2%)
    all_gather x1, waiting for transfers between devices, on_device(): down_full = lax.all_gather(down_weight, 'fs', axis=1, tiled=True)  168 us
    all_to_all x1, waiting for transfers between devices, patch_trace(): lax.all_to_all(jnp.stack(lax.axis_size(axis_id) * [payload]), axis_id, 0, 0)  85.1 us
    reduce_scatter x1, waiting for transfers between devices, on_device(): lax.psum_scatter(jnp.dot(spread, down_full, preferred_element_type=jnp.fl...  29.6 us
    all_gather x1, waiting for transfers between devices, on_device(): gathered = lax.all_gather(mixed_state, 'tp', axis=0, tiled=True)  22.7 us
    all_to_all x1, waiting for transfers between devices, on_device(): lax.all_to_all(hidden_first, 'tp', split_axis=1, concat_axis=0, tiled=True)  17.4 us
    dot_general x1, matrix products, on_device(): jnp.dot(gathered, patch_trace('fs', payload=joined), preferred_element_ty...  10.1 us
  transfers between devices with their start and end apart: 5, of which 5 were waited for; matrix products, arithmetic and copies ran while one was open for 6% of the time, Pallas kernels for 0%

profile of v1, /device:TPU:0, one launch (start us, length us, event | category | flops | bytes accessed | tf_op | source)
XLA Modules:
  0.0 384.2 jit_solution(12662064610168555700)
XLA Ops:
  7.2 0.0 all-gather.3.cloned.1.call-start
  7.2 0.7 all-gather.3.cloned.1.call-update
  7.9 2.5 copy.10
  10.4 4.3 %all-to-all-start = ((bf16[128,4,1408]{0,2,1:T(8,128)(2,1)}), bf16[128,4,1408]{0,2,1:T(8,128)(2,1)}, u32[]{:S(2)}, u32[]{:S(2)}) async-start(bf16[128,4,1408]{0,2,1:T(8,128)(2,1)} %bitcast), calls=%async_computation | async-start | bytes 2883584 | tf_op jit(solution)/shard_map/all_to_all | solution.py:23
  14.8 2.0 pad_maximum_fusion
  16.8 17.4 %all-to-all-done = bf16[128,4,1408]{0,2,1:T(8,128)(2,1)} async-done(((bf16[128,4,1408]{0,2,1:T(8,128)(2,1)}), bf16[128,4,1408]{0,2,1:T(8,128)(2,1)}, u32[]{:S(2)}, u32[]{:S(2)}) %all-to-all-start) | async-done | bytes 1441824 | tf_op jit(solution)/shard_map/all_to_all | solution.py:23
  34.1 5.0 %stack.2 = bf16[4,512,2816]{2,1,0:T(8,128)(2,1)} broadcast(bf16[512,2816]{1,0:T(8,128)(2,1)S(1)} %pad_maximum_fusion), dimensions={1,2} | broadcast | bytes 14417920 | tf_op jit(solution)/shard_map/stack | solution.py:9
  39.1 6.2 %all-to-all-start.1 = ((bf16[4,512,2816]{2,1,0:T(8,128)(2,1)}), bf16[4,512,2816]{2,1,0:T(8,128)(2,1)}, u32[]{:S(2)}, u32[]{:S(2)}) async-start(bf16[4,512,2816]{2,1,0:T(8,128)(2,1)} %stack.2), calls=%async_computation.2 | async-start | bytes 23068672 | tf_op jit(solution)/shard_map/all_to_all | solution.py:9
  45.3 0.0 reduce-scatter.2.cloned.1.call-start
  45.3 1.8 copy.11
  47.1 167.9 %all-gather.3.cloned.1.call-done = bf16[1408,2048]{1,0:T(8,128)(2,1)} async-done(((bf16[1408,512]{1,0:T(8,128)(2,1)}), bf16[1408,2048]{1,0:T(8,128)(2,1)}) %all-gather.3.cloned.1.call-update) | async-done | bytes 5767184 | tf_op jit(solution)/shard_map/all_gather | solution.py:24
  215.0 0.0 copy-start.2
  215.0 0.0 copy-start.3
  215.0 0.0 copy-start
  215.0 7.3 %convolution_convert_fusion = bf16[512,2048]{1,0:T(8,128)(2,1)} fusion(bf16[512,1408]{1,0:T(8,128)(2,1)S(1)} %bitcast.12, bf16[1408,2048]{1,0:T(8,128)(2,1)} %all-gather.3.cloned.1.call-done), kind=kOutput, calls=%fused_computation | convolution fusion | flops 2953838592 | bytes 9306112 | tf_op jit(solution)/shard_map/dot_general | solution.py:26
  222.3 0.0 reduce-scatter.2.cloned.1.call-update
  222.3 0.0 all-gather.5.cloned.1.call-start
  222.4 0.0 copy-done.2
  222.4 0.0 copy-done.3
  222.4 29.6 %reduce-scatter.2.cloned.1.call-done = bf16[128,2048]{1,0:T(8,128)(2,1)} async-done(((bf16[512,2048]{1,0:T(8,128)(2,1)}), bf16[128,2048]{1,0:T(8,128)(2,1)}) %reduce-scatter.2.cloned.1.call-update) | async-done | bytes 524304 | tf_op jit(solution)/shard_map/reduce_scatter | solution.py:25
  252.0 0.0 copy-done
  252.0 1.3 fusion.1
  253.4 1.4 multiply_reduce_fusion.1
  254.8 0.0 copy-done.1
  254.8 1.6 fusion.2
  256.4 0.3 multiply_reduce_fusion
  256.7 1.1 add_convert_fusion
  257.7 0.0 all-gather.5.cloned.1.call-update
  257.7 22.7 %all-gather.5.cloned.1.call-done = bf16[512,2048]{1,0:T(8,128)(2,1)} async-done(((bf16[128,2048]{1,0:T(8,128)(2,1)}), bf16[512,2048]{1,0:T(8,128)(2,1)}) %all-gather.5.cloned.1.call-update) | async-done | bytes 2097168 | tf_op jit(solution)/shard_map/all_gather | solution.py:37
  280.4 85.1 %all-to-all-done.1 = bf16[4,512,2816]{2,1,0:T(8,128)(2,1)} async-done(((bf16[4,512,2816]{2,1,0:T(8,128)(2,1)}), bf16[4,512,2816]{2,1,0:T(8,128)(2,1)}, u32[]{:S(2)}, u32[]{:S(2)}) %all-to-all-start.1) | async-done | bytes 11534368 | tf_op jit(solution)/shard_map/all_to_all | solution.py:9
  365.6 10.1 %fusion.5 = f32[512,2816]{1,0:T(8,128)S(1)} fusion(bf16[512,2048]{1,0:T(8,128)(2,1)} %all-gather.5.cloned.1.call-done, bf16[2048,2816]{1,0:T(8,128)(2,1)} %bitcast.7), kind=kOutput, calls=%fused_computation.17 | convolution fusion | flops 5905580032 | bytes 19398656 | tf_op jit(solution)/shard_map/dot_general | solution.py:40
  375.7 2.0 fusion
  (7 shorter events, 0.1 us)
Async XLA Ops:
  7.2 207.8 %all-gather.3.cloned.1.call-start = ((), (), s32[]{:S(2)}) async-start(), calls=%async_computation.3 | async-start | bytes 7208960 | tf_op jit(solution)/shard_map/all_gather | solution.py:24
  10.4 23.7 %all-to-all-start = ((bf16[128,4,1408]{0,2,1:T(8,128)(2,1)}), bf16[128,4,1408]{0,2,1:T(8,128)(2,1)}, u32[]{:S(2)}, u32[]{:S(2)}) async-start(bf16[128,4,1408]{0,2,1:T(8,128)(2,1)} %bitcast), calls=%async_computation | async-start | bytes 2883584 | tf_op jit(solution)/shard_map/all_to_all | solution.py:23
  39.1 326.5 %all-to-all-start.1 = ((bf16[4,512,2816]{2,1,0:T(8,128)(2,1)}), bf16[4,512,2816]{2,1,0:T(8,128)(2,1)}, u32[]{:S(2)}, u32[]{:S(2)}) async-start(bf16[4,512,2816]{2,1,0:T(8,128)(2,1)} %stack.2), calls=%async_computation.2 | async-start | bytes 23068672 | tf_op jit(solution)/shard_map/all_to_all | solution.py:9
  45.3 206.8 %reduce-scatter.2.cloned.1.call-start = ((), (), s32[]{:S(2)}) async-start(), calls=%async_computation.4 | async-start | bytes 2621440 | tf_op jit(solution)/shard_map/reduce_scatter | solution.py:25
  215.0 7.3 %copy-start.2 = (f32[2,2048]{1,0:T(2,128)S(1)}, f32[2,2048]{1,0:T(2,128)}, u32[]{:S(2)}) copy-start(f32[2,2048]{1,0:T(2,128)} %param.12) | copy-start | bytes 49156
  215.0 7.4 %copy-start.3 = (f32[2,2048]{1,0:T(2,128)S(1)}, f32[2,2048]{1,0:T(2,128)}, u32[]{:S(2)}) copy-start(f32[2,2048]{1,0:T(2,128)} %param.13) | copy-start | bytes 49156
  215.0 37.0 %copy-start = (bf16[128,2048]{1,0:T(8,128)(2,1)S(1)}, bf16[128,2048]{1,0:T(8,128)(2,1)}, u32[]{:S(2)}) copy-start(bf16[128,2048]{1,0:T(8,128)(2,1)} %param.8) | copy-start | bytes 1572868
  222.3 32.5 %copy-start.1 = (bf16[128,2048]{1,0:T(8,128)(2,1)S(1)}, bf16[128,2048]{1,0:T(8,128)(2,1)}, u32[]{:S(2)}) copy-start(bf16[128,2048]{1,0:T(8,128)(2,1)} %param.11) | copy-start | bytes 1572868
  222.3 58.1 %all-gather.5.cloned.1.call-start = ((), (), s32[]{:S(2)}) async-start(), calls=%async_computation.5 | async-start | bytes 2621440 | tf_op jit(solution)/shard_map/all_gather | solution.py:37
Sparse Core Ops, SparseCore 0:
  9.5 205.4 all-gather.2
  222.4 29.5 reduce-scatter.1
  257.9 22.5 all-gather.4
